TPU v7x, 128 devices: a whole 4x4x4 slice. The times are simulated.
128 devices in a mesh: ra: 16 (over z, x), cb: 4 (over y), dp: 2 (over core).
Axes of the slice: x: 4, y: 4, z: 4, core: 2. Of those that a mesh axis runs over, the one named last changes fastest.
Arguments:
- carried: bfloat16 [3072, 4096], P('dp', 'ra'), may hold values from -100 to 100
- branch_in: bfloat16 [3072, 4096], P('dp', 'ra'), may hold values from -12 to 12
- gain_in: float32 [4096], P('ra'), may hold values from 0.1 to 1.9
- bias_in: float32 [4096], P('ra'), may hold values from -1.8 to 1.8
- up_weight: bfloat16 [4096, 16384], P('ra', 'cb'), may hold values from -0.125 to 0.125
- down_weight: bfloat16 [16384, 4096], P('cb', 'ra'), may hold values from -0.046875 to 0.046875
- gain_out: float32 [4096], P('ra'), may hold values from 0.1 to 1.9
- bias_out: float32 [4096], P('ra'), may hold values from -1.8 to 1.8
Outputs:
- layer_out: bfloat16 [3072, 4096], P('dp', 'ra')
All inputs are finite; a program needn't handle non-finite values.
Results may differ from a plain program's by a relative error of at most 0.006.
Values may be sent and summed in bfloat16 or wider, within the bound.
A program may use at most 64 MiB of HBM per device.

v0:
```python
import jax
import jax.numpy as jnp
from jax import lax
from jax.sharding import PartitionSpec as P

residual_scale = 2.0**0.25
norm_eps = 1e-05


def copy_for_each(array, axis):
    length = lax.axis_size(axis)
    return lax.all_to_all(
        jnp.broadcast_to(array[None], (length, *array.shape)), axis, 0, 0, tiled=True
    )


def of_everyone(array, axis):
    return copy_for_each(array, axis).sum(axis=0)


def packed_total(arrays, axis):
    ravelled, at, done = (jnp.concatenate([a.reshape(-1) for a in arrays]), 0, [])
    running = of_everyone(ravelled, axis)
    for a in arrays:
        done.append(running[at : at + a.size].reshape(a.shape))
        at += a.size
    return tuple(done)


def taken_together(array, axis):
    return copy_for_each(array, axis).astype(jnp.float32).sum(axis=0)


def normalize(mixed, totals, squares, width, gain, bias):
    mean = totals[:, None] / width
    spread = squares[:, None] / width - mean * mean
    return (mixed - mean) * lax.rsqrt(spread + norm_eps) * gain + bias


def per_device(carried, branch_in, gain_in, bias_in, up_weight, down_weight, gain_out, bias_out):
    width = carried.shape[1] * lax.axis_size("ra")
    mixed_in = residual_scale * carried.astype(jnp.float32) + branch_in.astype(jnp.float32)
    totals, squares = packed_total(
        (jnp.sum(mixed_in, axis=1), jnp.sum(mixed_in * mixed_in, axis=1)), "ra"
    )
    normed = normalize(mixed_in, totals, squares, width, gain_in, bias_in).astype(jnp.bfloat16)
    regrouped = lax.all_to_all(up_weight, "ra", split_axis=1, concat_axis=0, tiled=True)
    pre_share = lax.dot_general(
        regrouped,
        lax.all_gather(normed, "ra", axis=1, tiled=True),
        (((0,), (1,)), ((), ())),
        preferred_element_type=jnp.float32,
    )
    hidden_share = jnp.square(jnp.maximum(pre_share, 0.0)).astype(jnp.bfloat16)
    branch_part = lax.dot_general(
        lax.all_gather(hidden_share, "ra", axis=0, tiled=True),
        down_weight,
        (((0,), (0,)), ((), ())),
        preferred_element_type=jnp.float32,
    )
    branch_out = taken_together(branch_part.astype(jnp.bfloat16), "cb").astype(jnp.float32)
    mixed_out = residual_scale * normed.astype(jnp.float32) + branch_out
    totals_out, squares_out = packed_total(
        (jnp.sum(mixed_out, axis=1), jnp.sum(mixed_out * mixed_out, axis=1)), "ra"
    )
    return normalize(mixed_out, totals_out, squares_out, width, gain_out, bias_out).astype(
        jnp.bfloat16
    )


def solution(mesh):
    in_specs = (
        P("dp", "ra"),
        P("dp", "ra"),
        P("ra"),
        P("ra"),
        P("ra", "cb"),
        P("cb", "ra"),
        P("ra"),
        P("ra"),
    )
    out_specs = P("dp", "ra")
    return jax.shard_map(
        per_device, mesh=mesh, in_specs=in_specs, out_specs=out_specs, check_vma=False
    )
```

profile of v0, /device:TPU:0, one launch (start us, length us, event | category | flops | bytes accessed | tf_op | source)
XLA Modules:
  0.0 324.9 jit_solution(11136814874928397678)
XLA Ops:
  6.5 0.0 copy-start
  6.5 0.0 copy-start.3
  6.5 0.0 copy-start.4
  6.5 0.0 copy-start.5
  6.5 0.0 all-gather.3.cloned.1.call-start
  6.6 2.1 fusion.3
  8.7 0.1 broadcast_in_dim.6
  8.8 16.1 %all_to_all.36 = f32[16,1,3072]{2,1,0:T(1,128)S(1)} all-to-all(f32[16,1,3072]{2,1,0:T(1,128)S(1)} %broadcast_in_dim.6), channel_id=1, replica_groups=mesh['ra'=16,'cb'=4,'dp'=2] {'ra'}, dimensions={0} | all-to-all | bytes 393216 | tf_op jit(solution)/shard_map/all_to_all | solution.py:12
  24.9 0.1 reduce_sum.65
  25.1 0.0 copy-done.3
  25.1 0.0 copy-done.4
  25.1 0.0 copy-done.5
  25.1 2.5 add_convert_fusion.1
  27.6 0.0 all-gather.3.cloned.1.call-update
  27.6 0.0 all-gather.5.cloned.1.call-start
  27.7 4.1 %copy.14 = bf16[256,4096]{0,1:T(8,128)(2,1)} copy(bf16[256,4096]{1,0:T(8,128)(2,1)} %param.12) | data formatting | bytes 4194304 | tf_op args[4]
  31.7 44.3 %all_to_all.37 = bf16[256,16,256]{0,2,1:T(8,128)(2,1)} all-to-all(bf16[256,16,256]{0,2,1:T(8,128)(2,1)} %bitcast.10), channel_id=1, replica_groups=mesh['ra'=16,'cb'=4,'dp'=2] {'ra'}, dimensions={1} | all-to-all | bytes 4194304 | tf_op jit(solution)/shard_map/all_to_all | solution.py:47
  76.0 3.9 %copy.15 = bf16[16,256,256]{2,1,0:T(8,128)(2,1)} copy(bf16[16,256,256]{1,2,0:T(8,128)(2,1)} %bitcast.9) | data formatting | bytes 4194304 | tf_op jit(solution)/shard_map/all_to_all | solution.py:47
  79.9 65.2 %all-gather.3.cloned.1.call-done = bf16[1536,4096]{1,0:T(8,128)(2,1)} async-done(((bf16[1536,256]{1,0:T(8,128)(2,1)}), bf16[1536,4096]{1,0:T(8,128)(2,1)}) %all-gather.3.cloned.1.call-update) | async-done | bytes 12582928 | tf_op jit(solution)/shard_map/all_gather | solution.py:50
  145.1 9.6 %fusion.2 = bf16[256,1536]{0,1:T(8,128)(2,1)} fusion(bf16[1536,4096]{1,0:T(8,128)(2,1)} %all-gather.3.cloned.1.call-done, bf16[4096,256]{1,0:T(8,128)(2,1)} %bitcast.11), kind=kOutput, calls=%fused_computation.5 | convolution fusion | flops 3222405120 | bytes 15466496 | tf_op jit(solution)/shard_map/dot_general | solution.py:48
  154.7 0.0 all-gather.5.cloned.1.call-update
  154.7 98.0 %all-gather.5.cloned.1.call-done = bf16[4096,1536]{0,1:T(8,128)(2,1)} async-done(((bf16[256,1536]{0,1:T(8,128)(2,1)}), bf16[4096,1536]{0,1:T(8,128)(2,1)}) %all-gather.5.cloned.1.call-update) | async-done | bytes 12582928 | tf_op jit(solution)/shard_map/all_gather | solution.py:56
  252.8 0.0 copy-done
  252.8 6.5 %convolution_convert_fusion = bf16[1536,256]{1,0:T(8,128)(2,1)S(1)} fusion(bf16[4096,1536]{0,1:T(8,128)(2,1)} %all-gather.5.cloned.1.call-done, bf16[4096,256]{1,0:T(8,128)(2,1)S(1)} %copy-done), kind=kOutput, calls=%fused_computation.4 | convolution fusion | flops 3221618688 | bytes 15466496 | tf_op jit(solution)/shard_map/dot_general | solution.py:55
  259.3 0.2 broadcast_in_dim.7
  259.5 40.3 %all_to_all.38 = bf16[4,1536,256]{2,1,0:T(8,128)(2,1)S(1)} all-to-all(bf16[4,1536,256]{2,1,0:T(8,128)(2,1)S(1)} %broadcast_in_dim.7), channel_id=1, replica_groups=mesh['ra'=16,'cb'=4,'dp'=2] {'cb'}, dimensions={0} | all-to-all | bytes 6291456 | tf_op jit(solution)/shard_map/all_to_all | solution.py:12
  299.8 0.0 copy-start.2
  299.8 0.5 convert_reduce_fusion
  300.2 0.0 copy-start.1
  300.2 1.1 copy-done.1
  301.4 0.0 copy-done.2
  301.4 0.0 copy-start.6
  301.4 0.0 copy-start.7
  301.4 0.5 fusion.4
  301.9 0.1 broadcast_in_dim.8
  302.0 13.1 %all_to_all.39 = f32[16,1,3072]{2,1,0:T(1,128)S(1)} all-to-all(f32[16,1,3072]{2,1,0:T(1,128)S(1)} %broadcast_in_dim.8), channel_id=1, replica_groups=mesh['ra'=16,'cb'=4,'dp'=2] {'ra'}, dimensions={0} | all-to-all | bytes 393216 | tf_op jit(solution)/shard_map/all_to_all | solution.py:12
  315.1 0.1 reduce_sum.69
  315.3 0.0 copy-done.6
  315.3 0.0 copy-done.7
  315.3 2.8 add_convert_fusion
  (4 shorter events, 0.0 us)
Async XLA Ops:
  6.5 246.2 %copy-start = (bf16[4096,256]{1,0:T(8,128)(2,1)S(1)}, bf16[4096,256]{1,0:T(8,128)(2,1)}, u32[]{:S(2)}) copy-start(bf16[4096,256]{1,0:T(8,128)(2,1)} %param.13) | copy-start | bytes 6291460
  6.5 18.5 %copy-start.3 = (bf16[1536,256]{1,0:T(8,128)(2,1)S(1)}, bf16[1536,256]{1,0:T(8,128)(2,1)}, u32[]{:S(2)}) copy-start(bf16[1536,256]{1,0:T(8,128)(2,1)} %param.9) | copy-start | bytes 2359300
  6.5 18.5 %copy-start.4 = (f32[256]{0:T(256)S(1)}, f32[256]{0:T(256)}, u32[]{:S(2)}) copy-start(f32[256]{0:T(256)} %param.11) | copy-start | bytes 3076
  6.5 18.5 %copy-start.5 = (f32[256]{0:T(256)S(1)}, f32[256]{0:T(256)}, u32[]{:S(2)}) copy-start(f32[256]{0:T(256)} %param.10) | copy-start | bytes 3076
  6.5 138.6 %all-gather.3.cloned.1.call-start = ((), (), s32[]{:S(2)}) async-start(), calls=%async_computation.4 | async-start | bytes 13369344 | tf_op jit(solution)/shard_map/all_gather | solution.py:50
  27.6 225.1 %all-gather.5.cloned.1.call-start = ((), (), s32[]{:S(2)}) async-start(), calls=%async_computation.5 | async-start | bytes 13369344 | tf_op jit(solution)/shard_map/all_gather | solution.py:56
  299.8 1.6 copy-start.2
  300.2 1.2 copy-start.1
  301.4 13.9 %copy-start.6 = (f32[256]{0:T(256)S(1)}, f32[256]{0:T(256)}, u32[]{:S(2)}) copy-start(f32[256]{0:T(256)} %param.15) | copy-start | bytes 3076
  301.4 13.9 %copy-start.7 = (f32[256]{0:T(256)S(1)}, f32[256]{0:T(256)}, u32[]{:S(2)}) copy-start(f32[256]{0:T(256)} %param.14) | copy-start | bytes 3076
Sparse Core Ops, SparseCore 0:
  27.7 117.3 all-gather.2
  154.9 97.8 all-gather.4
where the time goes:
time: 325 us
  waiting for transfers between devices  163 us (50%)
  blocking collectives  114 us (35%)
  matrix products  16.1 us (5%)
  between operations  13.5 us (4%)
  local copies, waits for them, and re-layouts  9.57 us (3%)
  other arithmetic  8.59 us (3%)
    all_gather x1, waiting for transfers between devices, per_device(): lax.all_gather(hidden_share, 'ra', axis=0, tiled=True)  98 us
    all_to_all x3, blocking collectives, copy_for_each(): lax.all_to_all(jnp.broadcast_to(array[None], (length, *array.shape)), axi...  69.5 us
    all_gather x1, waiting for transfers between devices, per_device(): lax.all_gather(normed, 'ra', axis=1, tiled=True)  65.2 us
    all_to_all x1, blocking collectives, per_device(): lax.all_to_all(up_weight, 'ra', split_axis=1, concat_axis=0, tiled=True)  44.3 us
    dot_general x1, matrix products, per_device(): lax.dot_general(regrouped, lax.all_gather(normed, 'ra', axis=1, tiled=Tru...  9.57 us
  transfers between devices with their start and end apart: 2, of which 2 were waited for; matrix products, arithmetic and copies ran while one was open for 2% of the time, Pallas kernels for 0%

commit v1 on v0

--- a/solution.py
+++ b/solution.py
@@ -53,7 +53,9 @@
     )
     hidden_share = jnp.square(jnp.maximum(pre_share, 0.0)).astype(jnp.bfloat16)
     branch_part = lax.dot_general(
-        lax.all_gather(hidden_share, "ra", axis=0, tiled=True),
+        jnp.concatenate(
+            lax.all_to_all(jnp.stack([hidden_share] * lax.axis_size("ra")), "ra", 0, 0), axis=0
+        ),
         down_weight,
         (((0,), (0,)), ((), ())),
         preferred_element_type=jnp.float32,

time: 325 us -> 378 us (1.16)
  blocking collectives: 114 us -> 260 us
  waiting for transfers between devices: 163 us -> 65.2 us
  local copies, waits for them, and re-layouts: 9.57 us -> 16.8 us
    all_to_all x0 -> x1, blocking collectives: none -> 147 us  [per_device(): lax.all_to_all(jnp.stack([hidden_share] * lax.axis_size('ra')), 'ra', 0, 0)]
    all_gather x1 -> x0, waiting for transfers between devices: 98 us -> none  [per_device(): lax.all_gather(hidden_share, 'ra', axis=0, tiled=True)]
    another operation x0 -> x1, local copies, waits for them, and re-layouts: none -> 5.78 us  [per_device(): jnp.stack([hidden_share] * lax.axis_size('ra'))]
  transfers between devices with their start and end apart: 2 -> 1, of which waited for: 2 -> 1; matrix products, arithmetic and copies ran while one was open for 2% -> 2% of each run, Pallas kernels for 0% -> 0%
where the time goes in v1:
time: 378 us; the launch traced here: 377 us
  blocking collectives  260 us (69%)
  waiting for transfers between devices  65.2 us (17%)
  local copies, waits for them, and re-layouts  16.8 us (4%)
  between operations  13.5 us (4%)
  matrix products  13.3 us (4%)
  other arithmetic  8.59 us (2%)
    all_to_all x1, blocking collectives, per_device(): lax.all_to_all(jnp.stack([hidden_share] * lax.axis_size('ra')), 'ra', 0, 0)  147 us
    all_to_all x3, blocking collectives, copy_for_each(): lax.all_to_all(jnp.broadcast_to(array[None], (length, *array.shape)), axi...  68 us
    all_gather x1, waiting for transfers between devices, per_device(): lax.all_gather(normed, 'ra', axis=1, tiled=True)  65.2 us
    all_to_all x1, blocking collectives, per_device(): lax.all_to_all(up_weight, 'ra', split_axis=1, concat_axis=0, tiled=True)  44.3 us
    dot_general x1, matrix products, per_device(): lax.dot_general(regrouped, lax.all_gather(normed, 'ra', axis=1, tiled=Tru...  9.58 us
  transfers between devices with their start and end apart: 1, of which 1 were waited for; matrix products, arithmetic and copies ran while one was open for 2% of the time, Pallas kernels for 0%

profile of v1, /device:TPU:0, one launch (start us, length us, event | category | flops | bytes accessed | tf_op | source)
XLA Modules:
  0.0 377.0 jit_solution(10895604707394252497)
XLA Ops:
  6.5 0.0 copy-start
  6.5 0.0 copy-start.3
  6.5 0.0 copy-start.4
  6.5 0.0 copy-start.5
  6.5 0.0 all-gather.2.cloned.1.call-start
  6.6 2.1 fusion.3
  8.7 0.1 broadcast_in_dim.6
  8.8 16.1 %all_to_all.41 = f32[16,1,3072]{2,1,0:T(1,128)S(1)} all-to-all(f32[16,1,3072]{2,1,0:T(1,128)S(1)} %broadcast_in_dim.6), channel_id=1, replica_groups=mesh['ra'=16,'cb'=4,'dp'=2] {'ra'}, dimensions={0} | all-to-all | bytes 393216 | tf_op jit(solution)/shard_map/all_to_all | solution.py:12
  24.9 0.1 reduce_sum.65
  25.1 0.0 copy-done.3
  25.1 0.0 copy-done.4
  25.1 0.0 copy-done.5
  25.1 2.5 add_convert_fusion.1
  27.6 0.0 all-gather.2.cloned.1.call-update
  27.6 4.1 %copy.18 = bf16[256,4096]{0,1:T(8,128)(2,1)} copy(bf16[256,4096]{1,0:T(8,128)(2,1)} %param.12) | data formatting | bytes 4194304 | tf_op args[4]
  31.7 44.3 %all_to_all.42 = bf16[256,16,256]{0,2,1:T(8,128)(2,1)} all-to-all(bf16[256,16,256]{0,2,1:T(8,128)(2,1)} %bitcast.12), channel_id=1, replica_groups=mesh['ra'=16,'cb'=4,'dp'=2] {'ra'}, dimensions={1} | all-to-all | bytes 4194304 | tf_op jit(solution)/shard_map/all_to_all | solution.py:47
  76.0 3.9 %copy.19 = bf16[16,256,256]{2,1,0:T(8,128)(2,1)} copy(bf16[16,256,256]{1,2,0:T(8,128)(2,1)} %bitcast.11) | data formatting | bytes 4194304 | tf_op jit(solution)/shard_map/all_to_all | solution.py:47
  79.9 65.2 %all-gather.2.cloned.1.call-done = bf16[1536,4096]{1,0:T(8,128)(2,1)} async-done(((bf16[1536,256]{1,0:T(8,128)(2,1)}), bf16[1536,4096]{1,0:T(8,128)(2,1)}) %all-gather.2.cloned.1.call-update) | async-done | bytes 12582928 | tf_op jit(solution)/shard_map/all_gather | solution.py:50
  145.1 9.6 %fusion.2 = bf16[256,1536]{0,1:T(8,128)(2,1)} fusion(bf16[1536,4096]{1,0:T(8,128)(2,1)} %all-gather.2.cloned.1.call-done, bf16[4096,256]{1,0:T(8,128)(2,1)} %bitcast.13), kind=kOutput, calls=%fused_computation.5 | convolution fusion | flops 3222405120 | bytes 15466496 | tf_op jit(solution)/shard_map/dot_general | solution.py:48
  154.7 1.4 copy.20
  156.1 5.8 %stack.2 = bf16[16,256,1536]{2,1,0:T(8,128)(2,1)} broadcast(bf16[256,1536]{1,0:T(8,128)(2,1)S(1)} %copy.20), dimensions={1,2} | broadcast | bytes 13369344 | tf_op jit(solution)/shard_map/stack | solution.py:57
  161.9 147.3 %all_to_all.43 = bf16[16,256,1536]{2,1,0:T(8,128)(2,1)S(1)} all-to-all(bf16[16,256,1536]{2,1,0:T(8,128)(2,1)} %stack.2), channel_id=1, replica_groups=mesh['ra'=16,'cb'=4,'dp'=2] {'ra'}, dimensions={0} | all-to-all | bytes 25165824 | tf_op jit(solution)/shard_map/all_to_all | solution.py:57
  309.2 0.0 copy-done
  309.2 3.7 convolution_convert_fusion
  312.9 0.2 broadcast_in_dim.7
  313.1 38.5 %all_to_all.44 = bf16[4,1536,256]{2,1,0:T(8,128)(2,1)S(1)} all-to-all(bf16[4,1536,256]{2,1,0:T(8,128)(2,1)S(1)} %broadcast_in_dim.7), channel_id=1, replica_groups=mesh['ra'=16,'cb'=4,'dp'=2] {'cb'}, dimensions={0} | all-to-all | bytes 6291456 | tf_op jit(solution)/shard_map/all_to_all | solution.py:12
  351.6 0.0 copy-start.2
  351.6 0.5 convert_reduce_fusion
  352.1 0.0 copy-start.1
  352.1 1.1 copy-done.1
  353.2 0.0 copy-done.2
  353.2 0.0 copy-start.6
  353.2 0.0 copy-start.7
  353.2 0.5 fusion.4
  353.8 0.1 broadcast_in_dim.8
  353.9 13.4 %all_to_all.45 = f32[16,1,3072]{2,1,0:T(1,128)S(1)} all-to-all(f32[16,1,3072]{2,1,0:T(1,128)S(1)} %broadcast_in_dim.8), channel_id=1, replica_groups=mesh['ra'=16,'cb'=4,'dp'=2] {'ra'}, dimensions={0} | all-to-all | bytes 393216 | tf_op jit(solution)/shard_map/all_to_all | solution.py:12
  367.2 0.1 reduce_sum.69
  367.4 0.0 copy-done.6
  367.4 0.0 copy-done.7
  367.4 2.8 add_convert_fusion
  (4 shorter events, 0.0 us)
Async XLA Ops:
  6.5 302.7 %copy-start = (bf16[4096,256]{1,0:T(8,128)(2,1)S(1)}, bf16[4096,256]{1,0:T(8,128)(2,1)}, u32[]{:S(2)}) copy-start(bf16[4096,256]{1,0:T(8,128)(2,1)} %param.13) | copy-start | bytes 6291460
  6.5 18.5 %copy-start.3 = (bf16[1536,256]{1,0:T(8,128)(2,1)S(1)}, bf16[1536,256]{1,0:T(8,128)(2,1)}, u32[]{:S(2)}) copy-start(bf16[1536,256]{1,0:T(8,128)(2,1)} %param.9) | copy-start | bytes 2359300
  6.5 18.5 %copy-start.4 = (f32[256]{0:T(256)S(1)}, f32[256]{0:T(256)}, u32[]{:S(2)}) copy-start(f32[256]{0:T(256)} %param.11) | copy-start | bytes 3076
  6.5 18.5 %copy-start.5 = (f32[256]{0:T(256)S(1)}, f32[256]{0:T(256)}, u32[]{:S(2)}) copy-start(f32[256]{0:T(256)} %param.10) | copy-start | bytes 3076
  6.5 138.5 %all-gather.2.cloned.1.call-start = ((), (), s32[]{:S(2)}) async-start(), calls=%async_computation.5 | async-start | bytes 13369344 | tf_op jit(solution)/shard_map/all_gather | solution.py:50
  351.6 1.6 copy-start.2
  352.1 1.2 copy-start.1
  353.2 14.2 %copy-start.6 = (f32[256]{0:T(256)S(1)}, f32[256]{0:T(256)}, u32[]{:S(2)}) copy-start(f32[256]{0:T(256)} %param.15) | copy-start | bytes 3076
  353.2 14.2 %copy-start.7 = (f32[256]{0:T(256)S(1)}, f32[256]{0:T(256)}, u32[]{:S(2)}) copy-start(f32[256]{0:T(256)} %param.14) | copy-start | bytes 3076
Sparse Core Ops, SparseCore 0:
  27.7 117.3 all-gather.1
